TPU v7x, 32 devices: a whole 2x2x4 slice. The times are simulated.
32 devices in a mesh: sp: 8 (over z, y), tp: 4 (over x, core).
Axes of the slice: x: 2, y: 2, z: 4, core: 2. Of those that a mesh axis runs over, the one named last changes fastest.
Arguments:
- stream: bfloat16 [8192, 2048], P(('sp', 'tp')), may hold values from -6 to 6
- query_rows: bfloat16 [8192, 1024], P('sp', 'tp'), may hold values from -6 to 6
- key_rows: bfloat16 [8192, 1024], P('sp', 'tp'), may hold values from -6 to 6
- value_rows: bfloat16 [8192, 2048], P('sp', 'tp'), may hold values from -6 to 6
- gate_rows: bfloat16 [8192, 2048], P('sp', 'tp'), may hold values from -6 to 6
- log_decay: float32 [8192, 1024], P('sp', 'tp'), may hold values from -1 to 0
- head_gain: float32 [256], replicated, may hold values from 0.1 to 1.9
- out_weight: bfloat16 [2048, 2048], P('tp'), may hold values from -0.125 to 0.125
- mix_gain: float32 [2048], replicated, may hold values from 0.1 to 1.9
- up_weight: bfloat16 [2048, 8192], P('sp', 'tp'), may hold values from -0.125 to 0.125
- down_weight: bfloat16 [2048, 8192], P('sp', 'tp'), may hold values from -0.0625 to 0.0625
Outputs:
- mixed_out: bfloat16 [8192, 2048], P(('sp', 'tp'))
All inputs are finite; a program needn't handle non-finite values.
Results may differ from a plain program's by a relative error of at most 0.02.
Values may be sent and summed in bfloat16 or wider, within the bound.
A program may use at most 128 MiB of HBM per device.

v0:
```python
import functools

import jax
import jax.numpy as jnp
from jax import lax
from jax.experimental import pallas as pl
from jax.experimental.pallas import tpu as pltpu
from jax.sharding import PartitionSpec as P


KEY_CHANNELS = 128
DV = 256
BLOCK = 64
EPS = 1e-06


NT = (((1,), (1,)), ((), ()))
TN = (((0,), (0,)), ((), ()))


def local_states(q_ref, k_ref, v_ref, ld_ref, out_ref, qd_ref, state_ref):
    count = q_ref.shape[0] // BLOCK
    row = lax.broadcasted_iota(jnp.int32, (BLOCK, BLOCK), 0)
    col = lax.broadcasted_iota(jnp.int32, (BLOCK, BLOCK), 1)
    later = (col > row).astype(jnp.float32)
    scale = KEY_CHANNELS ** (-0.5)
    state = jnp.zeros((DV, KEY_CHANNELS), jnp.float32)
    total = jnp.zeros((1, KEY_CHANNELS), jnp.float32)
    for c in range(count):
        rows = pl.ds(c * BLOCK, BLOCK)
        rates = ld_ref[rows, :]
        rest = jnp.dot(later, rates, precision=lax.Precision.HIGHEST, preferred_element_type=jnp.float32)
        last = jnp.sum(rates, axis=0, keepdims=True)
        keys = (k_ref[rows, :].astype(jnp.float32) * jnp.exp(rest)).astype(jnp.bfloat16)
        update = lax.dot_general(v_ref[rows, :], keys, TN, preferred_element_type=jnp.float32)
        state = state * jnp.exp(last) + update
        total = total + last
        q = q_ref[rows, :]
        out_ref[rows, :] = lax.dot_general(
            q, state.astype(jnp.bfloat16), NT, preferred_element_type=jnp.float32
        ) * scale
        qd_ref[rows, :] = (q.astype(jnp.float32) * (jnp.exp(total) * scale)).astype(jnp.bfloat16)
    state_ref[0, :DV, :] = state.astype(jnp.bfloat16)
    state_ref[0, DV:, :] = jnp.broadcast_to(jnp.exp(total), (16, KEY_CHANNELS)).astype(jnp.bfloat16)


def finish_heads(own_ref, qd_ref, state_ref, gate_ref, gain_ref, out_ref):
    readout = own_ref[...] + lax.dot_general(
        qd_ref[...], state_ref[0, :DV, :], NT, preferred_element_type=jnp.float32
    )
    scaled = readout * lax.rsqrt(jnp.mean(readout * readout, axis=-1, keepdims=True) + EPS)
    gates = gate_ref[...].astype(jnp.float32)
    out_ref[...] = (scaled * gain_ref[...] * (gates / (1.0 + jnp.exp(-gates)))).astype(jnp.bfloat16)


def attention_local(q, k, v, ld):
    rows = q.shape[0]
    heads = q.shape[1] // KEY_CHANNELS
    kb = pl.BlockSpec((rows, KEY_CHANNELS), lambda h: (0, h))
    vb = pl.BlockSpec((rows, DV), lambda h: (0, h))
    return pl.pallas_call(
        local_states,
        grid=(heads,),
        in_specs=[kb, kb, vb, kb],
        out_specs=[vb, kb, pl.BlockSpec((1, DV + 16, KEY_CHANNELS), lambda h: (h, 0, 0))],
        out_shape=[
            jax.ShapeDtypeStruct((rows, heads * DV), jnp.float32),
            jax.ShapeDtypeStruct((rows, heads * KEY_CHANNELS), jnp.bfloat16),
            jax.ShapeDtypeStruct((heads, DV + 16, KEY_CHANNELS), jnp.bfloat16),
        ],
        cost_estimate=pl.CostEstimate(flops=6_000_000_000, bytes_accessed=8_000_000, transcendentals=0),
        name="local_states",
    )(q, k, v, ld)


def attention_finish(own, qd, state, gates, gain):
    rows = own.shape[0]
    heads = own.shape[1] // DV
    tile = rows // 2
    vb = pl.BlockSpec((tile, DV), lambda h, r: (r, h))
    return pl.pallas_call(
        finish_heads,
        grid=(heads, rows // tile),
        in_specs=[
            vb,
            pl.BlockSpec((tile, KEY_CHANNELS), lambda h, r: (r, h)),
            pl.BlockSpec((1, DV + 16, KEY_CHANNELS), lambda h, r: (h, 0, 0)),
            vb,
            pl.BlockSpec((1, DV), lambda h, r: (0, 0)),
        ],
        out_specs=vb,
        out_shape=jax.ShapeDtypeStruct(own.shape, jnp.bfloat16),
        cost_estimate=pl.CostEstimate(flops=3_000_000_000, bytes_accessed=4_000_000, transcendentals=0),
        name="finish_heads",
    )(own, qd, state, gates, gain)


def join(earlier, later):
    e, f = earlier.astype(jnp.float32), later.astype(jnp.float32)
    decay = f[:, DV : DV + 1]
    return jnp.concatenate(
        [decay * e[:, :DV] + f[:, :DV], jnp.broadcast_to(decay * e[:, DV : DV + 1], e[:, DV:].shape)], axis=1
    ).astype(jnp.bfloat16)


def shifted(a, by, n):
    return lax.ppermute(a, "sp", [(i, i + by) for i in range(n - by)])


def cycle_of(n):
    return list(range(0, n, 2)) + list(range(n - 1 - n % 2, 0, -2))


class Ring:
    def __init__(self, piece, n):
        self.n, self.cyc, self.piece = n, cycle_of(n), piece
        self.fwd = [(self.cyc[i], self.cyc[(i + 1) % n]) for i in range(n)]
        self.bwd = [(b, a) for a, b in self.fwd]
        self.left = self.right = piece
        self.hops = n // 2

    def hop(self, h):
        left, right = self.left, self.right
        if h == self.hops:
            half = self.piece.shape[0] // 2
            left, right = left[:half], right[half:]
        self.left = lax.ppermute(left, "sp", self.fwd)
        self.right = lax.ppermute(right, "sp", self.bwd)
        if h == self.hops:
            return [jnp.concatenate([self.left, self.right], axis=0)]
        return [self.left, self.right]


def owner_of(n, h):
    cyc = cycle_of(n)
    place = [0] * n
    for i, d in enumerate(cyc):
        place[d] = i
    me = jnp.asarray(place, jnp.int32)[lax.axis_index("sp")]
    cyc = jnp.asarray(cyc, jnp.int32)
    if h == 0:
        return [cyc[me]]
    back = cyc[(me - h) % n]
    return [back] if 2 * h == n else [back, cyc[(me + h) % n]]


def local(
    n_sp, n_tp, stream, query_rows, key_rows, value_rows, gate_rows, log_decay, head_gain, out_weight, mix_gain,
    up_weight, down_weight,
):
    nx = n_tp // 2
    own_rows = stream.shape[0]
    me = lax.axis_index("tp")
    x, core = me // 2, me % 2

    def across(a, dx):
        return lax.ppermute(a, "tp", [(((i // 2 + dx) % nx) * 2 + i % 2, i) for i in range(n_tp)])

    def swap(a):
        return lax.ppermute(a, "tp", [(i ^ 1, i) for i in range(n_tp)])

    up = Ring(up_weight, n_sp)
    down = Ring(down_weight, n_sp)
    width = up_weight.shape[0]
    up_full = lax.dynamic_update_slice_in_dim(
        jnp.zeros((width * n_sp, up_weight.shape[1]), up_weight.dtype), up_weight, owner_of(n_sp, 0)[0] * width, 0
    )
    ups = [up.hop(1)]
    downs = [[down_weight]]

    def tie(a, ring):
        a, ring.left, ring.right = lax.optimization_barrier((a, ring.left, ring.right))
        return a

    w = {(0, 0): out_weight}
    for dx in range(1, nx):
        w[dx, 0] = across(out_weight, dx)
    for dx in range(nx):
        w[dx, 1] = swap(w[dx, 0])

    own, qd, summary = attention_local(query_rows, key_rows, value_rows, log_decay)
    before, covered = tie(shifted(summary, 1, n_sp), up), 1
    while covered < n_sp - 1:
        wider = join(before, summary)
        if len(ups) < up.hops - 1:
            ups.append(up.hop(len(ups) + 1))
        before, covered = join(shifted(wider, covered + 1, n_sp), before), 2 * covered + 1
        before = tie(before, up)
    while len(ups) < up.hops:
        ups.append(up.hop(len(ups) + 1))
    before, down.left, down.right = lax.optimization_barrier((before, down.left, down.right))
    downs.append(down.hop(1))
    heads_out = attention_finish(own, qd, before, gate_rows, head_gain.reshape(1, DV))

    attn = None
    for dx in range(nx):
        for dc in range(2):
            to = ((x - dx) % nx) * 2 + (core + dc) % 2
            block = lax.dynamic_slice_in_dim(heads_out, to * own_rows, own_rows, 0)
            if (dx, dc) != (0, 0):
                block = lax.ppermute(
                    block, "tp", [(((i // 2 + dx) % nx) * 2 + (i % 2 + dc) % 2, i) for i in range(n_tp)]
                )
            term = jnp.dot(block, w[dx, dc], preferred_element_type=jnp.float32)
            attn = term if attn is None else attn + term
    midf = (stream.astype(jnp.float32) + attn).astype(jnp.bfloat16).astype(jnp.float32)
    normed = (
        midf * lax.rsqrt(jnp.mean(midf * midf, axis=-1, keepdims=True) + EPS) * mix_gain
    ).astype(jnp.bfloat16)

    normed = tie(normed, down)
    downs.append(down.hop(2))

    for h, pieces in enumerate(ups, 1):
        for piece, who in zip(pieces, owner_of(n_sp, h)):
            up_full = lax.dynamic_update_slice_in_dim(up_full, piece, who * width, 0)

    n = {(0, 0): normed}
    for dx in range(1, nx):
        n[dx, 0] = across(normed, dx)
    for dx in range(nx):
        n[dx, 1] = swap(n[dx, 0])
    n[nx - 1, 1] = tie(n[nx - 1, 1], down)
    while len(downs) <= down.hops:
        downs.append(down.hop(len(downs)))
    order = [(dx, dc) for dc in range(2) for dx in range(nx)]

    def hidden_of(rows):
        pre = jnp.dot(rows, up_full, preferred_element_type=jnp.float32)
        return jnp.square(jax.nn.relu(pre)).astype(jnp.bfloat16)

    hiddens = []
    for key in order:
        hiddens.append(hidden_of(n[key]))
    hidden = jnp.concatenate(hiddens, axis=0)

    out = jnp.zeros(stream.shape, jnp.bfloat16)
    mid = midf.astype(jnp.bfloat16)
    for h, pieces in enumerate(downs):
        whole = jnp.concatenate(pieces, axis=0) if len(pieces) > 1 else pieces[0]
        part = lax.dot_general(hidden, whole, NT, preferred_element_type=jnp.float32).astype(jnp.bfloat16)
        hidden, part = lax.optimization_barrier((hidden, part))
        half = nx * own_rows
        both = part[:half].astype(jnp.float32) + swap(part[half:]).astype(jnp.float32)
        feed = both[:own_rows]
        for dx in range(1, nx):
            send = both[dx * own_rows : (dx + 1) * own_rows].astype(jnp.bfloat16)
            feed = feed + across(send, nx - dx).astype(jnp.float32)
        for j, who in enumerate(owner_of(n_sp, h)):
            cols = lax.dynamic_slice_in_dim(mid, who * width, width, 1).astype(jnp.float32)
            done = (cols + feed[:, j * width : (j + 1) * width]).astype(jnp.bfloat16)
            out = lax.dynamic_update_slice_in_dim(out, done, who * width, 1)
    return out


TILE = 256
MESH = pl.DeviceIdType.MESH


class Links:
    def __init__(self, n_sp):
        self.sp, self.tp = lax.axis_index("sp"), lax.axis_index("tp")
        self.nz = n_sp // 2
        self.z, self.y = self.sp // 2, self.sp % 2
        self.x, self.c = self.tp // 2, self.tp % 2
        self.core = (self.sp, self.x * 2 + 1 - self.c)
        self.xn = (self.sp, (1 - self.x) * 2 + self.c)
        self.xo = (self.sp, (1 - self.x) * 2 + 1 - self.c)
        self.yn = (self.z * 2 + 1 - self.y, self.tp)

    def at_z(self, z):
        return (z * 2 + self.y, self.tp)

    def piece(self, s):
        z, n = self.z, self.nz
        near = jnp.minimum(z, n - 1 - z)
        turn = jnp.where(s % 2 == 1, z - (s + 1) // 2, z + s // 2)
        rest = jnp.where(z < n - 1 - z, s, n - 1 - s)
        return jnp.where(s <= 2 * near, turn, rest)


def remote(src, dst, send, recv, dev):
    return pltpu.make_async_remote_copy(
        src_ref=src, dst_ref=dst, send_sem=send, recv_sem=recv, device_id=dev, device_id_type=MESH
    )


def layer_kernel(
    n_sp, n_tp, stream, query, key, value, gate, rates_in, head_gain, mix_gain, out_w, up_w, down_w, out,
    up, down, wo, qv, kv, vv, gv, ldv, own, qd, state, total, summ, peer, tsend, trecv, prefix, bsend, before,
    heads, hrecv, acts, hidden, mid, psend, pown, sum_x, sum_y, pass_y, pass_x, outv,
    ld_s, zown_s, zfwd_s, z_r, y_s, y_r, d_s, d_r, wo_s, wo_r, s_s, s_r, t_s, t_r, h_s, h_r, a_s, a_r, p_s, p_r, o_s,
):
    f32, bf16 = jnp.float32, jnp.bfloat16
    L = Links(n_sp)
    z, y, c, nz = L.z, L.y, L.c, L.nz
    rows, width = stream.shape
    span = query.shape[0]
    n_heads = query.shape[1] // KEY_CHANNELS
    slab, half = up_w.shape[0], up_w.shape[1] // 2
    half_rows = rows // 2
    np_ = 2 * nz

    loads = [(query, qv), (key, kv), (value, vv), (rates_in, ldv)]
    first = [pltpu.make_async_copy(a, b, ld_s.at[i]) for i, (a, b) in enumerate(loads)]
    for cp in first:
        cp.start()
    barrier = pltpu.get_barrier_semaphore()
    partners = [L.core, L.xn, L.xo, L.yn] + [L.at_z((z + k) % nz) for k in range(1, nz)]
    for dev in partners:
        pl.semaphore_signal(barrier, inc=1, device_id=dev, device_id_type=MESH)
    pl.semaphore_wait(barrier, len(partners))

    bufs, source = (up, down), (up_w, down_w)

    def place(kind, core, j, part):
        row = j * 2 + (part if kind else (y + part) % 2)
        return bufs[kind].at[core, pl.ds(pl.multiple_of(row * slab, slab), slab), :]

    def halfcols(kind, h):
        return source[kind].at[:, pl.ds(pl.multiple_of(h * half, half), half)]

    def own_rows(kind, yy):
        return bufs[kind].at[c, pl.ds(pl.multiple_of((z * 2 + yy) * slab, slab), slab), :]

    keep = [pltpu.make_async_copy(halfcols(k, y), own_rows(k, y), ld_s.at[6 + k]) for k in range(2)]
    cross = [
        remote(halfcols(k, 1 - y), own_rows(k, y), y_s.at[k], y_r.at[k], L.yn) for k in range(2)
    ]

    def to_side(kind, part, side):
        to = z + (1 if side else -1)
        src = halfcols(0, y) if (kind, part) == (0, 0) else place(kind, c, z, part)
        return remote(src, place(kind, c, z, part), zown_s.at[kind, part, side], z_r.at[kind, z, part], L.at_z((to + nz) % nz))

    def to_core(kind, j, part, from_hbm=False):
        dst = place(kind, c, j, part)
        return remote(halfcols(kind, y) if from_hbm else dst, dst, d_s.at[kind, j, part], d_r.at[kind, j, part], L.core)

    def send_own(kind, part, sides=(0, 1)):
        for side in sides:
            @pl.when((z < nz - 1) if side else (z > 0))
            def _():
                to_side(kind, part, side).start()

    def open_part(part):
        if part == 0:
            keep[0].start()
        else:
            cross[0].wait_recv()
        to_core(0, z, part, part == 0).start()

    def onward(kind, j, part):
        to = jnp.where(j < z, z + 1, z - 1)
        dst = place(kind, c, j, part)
        return remote(dst, dst, zfwd_s.at[kind, j, part], z_r.at[kind, j, part], L.at_z((to + nz) % nz))

    inner = jnp.logical_and(z > 0, z < nz - 1)
    edge = jnp.logical_or(z == 0, z == nz - 1)

    def arrive(kind, s, part, forward):
        j = L.piece(s)
        cp = onward(kind, j, part)
        cp.wait_recv()
        if forward:
            cp.start()
        to_core(kind, j, part).start()

    def forward_inner(kind, s, part):
        @pl.when(inner)
        def _():
            arrive(kind, s, part, True)

    def from_core(kind, j, part):
        dst = place(kind, 1 - c, j, part)
        return remote(dst, dst, d_s.at[kind, j, part], d_r.at[kind, j, part], L.core)

    cross[0].start()
    send_own(0, 0)
    wo_own = pltpu.make_async_copy(out_w, wo.at[L.tp], ld_s.at[4])
    wo_x = remote(out_w, wo.at[L.tp], wo_s.at[0], wo_r.at[0], L.xn)
    wo_c = remote(out_w, wo.at[L.tp], wo_s.at[1], wo_r.at[1], L.core)
    wo_x.start()
    wo_c.start()
    wo_own.start()
    open_part(0)
    keep[1].start()
    late = [pltpu.make_async_copy(gate, gv, ld_s.at[5]), pltpu.make_async_copy(stream, mid, ld_s.at[8])]
    for cp in late:
        cp.start()

    row = lax.broadcasted_iota(jnp.int32, (BLOCK, BLOCK), 0)
    col = lax.broadcasted_iota(jnp.int32, (BLOCK, BLOCK), 1)
    later = (col > row).astype(f32)
    scale = KEY_CHANNELS ** (-0.5)
    state[...] = jnp.zeros_like(state)
    total[...] = jnp.zeros_like(total)
    for cp in first:
        cp.wait()

    def block(i, carry):
        at = pl.ds(pl.multiple_of(i * BLOCK, BLOCK), BLOCK)
        for h in range(n_heads):
            ks, vs = pl.ds(h * KEY_CHANNELS, KEY_CHANNELS), pl.ds(h * DV, DV)
            rates = ldv[at, ks]
            rest = jnp.dot(later, rates, precision=lax.Precision.HIGHEST, preferred_element_type=f32)
            last = jnp.sum(rates, axis=0, keepdims=True)
            keys = (kv[at, ks].astype(f32) * jnp.exp(rest)).astype(bf16)
            update = lax.dot_general(vv[at, vs], keys, TN, preferred_element_type=f32)
            new = state[h] * jnp.exp(last) + update
            state[h] = new
            tot = total[h] + last
            total[h] = tot
            q = qv[at, ks]
            own[at, vs] = lax.dot_general(q, new.astype(bf16), NT, preferred_element_type=f32) * scale
            qd[at, ks] = (q.astype(f32) * (jnp.exp(tot) * scale)).astype(bf16)
        return carry

    lax.fori_loop(0, span // BLOCK, block, 0, unroll=2)
    for h in range(n_heads):
        summ[h, :DV, :] = state[h].astype(bf16)
        summ[h, DV:, :] = jnp.broadcast_to(jnp.exp(total[h]), (16, KEY_CHANNELS)).astype(bf16)

    swap = remote(summ.at[1 - y], peer, s_s.at[0], s_r.at[0], L.yn)
    swap.start()
    open_part(1)
    send_own(0, 1)
    swap.wait_recv()
    mine, other = summ[y].astype(f32), peer[...].astype(f32)
    is0 = y == 0
    early, late_ = jnp.where(is0, mine, other), jnp.where(is0, other, mine)
    dec = late_[DV : DV + 1]
    tsend[:DV, :] = (dec * early[:DV] + late_[:DV]).astype(bf16)
    tsend[DV:, :] = (dec * early[DV:]).astype(bf16)

    def hand_on(zz):
        return remote(tsend, trecv.at[z], t_s.at[zz], t_r.at[z], L.at_z(zz))

    for zz in range(1, nz):
        @pl.when(z < zz)
        def _():
            hand_on(zz).start()
    forward_inner(0, 1, 0)
    forward_inner(0, 2, 0)
    prefix[...] = jnp.zeros_like(prefix)
    for j in range(nz - 1):
        @pl.when(j < z)
        def _():
            remote(tsend, trecv.at[j], t_s.at[j], t_r.at[j], L.at_z(j)).wait_recv()
            got = trecv[j].astype(f32)
            prefix[...] = got[DV : DV + 1] * prefix[...] + got[:DV]
    whole = prefix[...]
    first_y = jnp.where(is0, mine, other)
    onto = first_y[DV : DV + 1] * whole + first_y[:DV]
    bsend[...] = jnp.where(is0, onto, whole).astype(bf16)
    before[y] = jnp.where(is0, whole, onto).astype(bf16)
    back = remote(bsend, before.at[y], s_s.at[1], s_r.at[1], L.yn)
    back.start()
    forward_inner(0, 1, 1)
    forward_inner(0, 2, 1)
    remote(bsend, before.at[1 - y], s_s.at[1], s_r.at[1], L.yn).wait_recv()
    cross[1].start()

    late[0].wait()
    gain = head_gain[...]

    def finish(t):
        for r in range(0, rows, 128):
            at = pl.ds(pl.multiple_of(t * rows + r, 128), 128)
            for h in range(n_heads):
                ks, vs = pl.ds(h * KEY_CHANNELS, KEY_CHANNELS), pl.ds(h * DV, DV)
                readout = own[at, vs] + lax.dot_general(qd[at, ks], before[h], NT, preferred_element_type=f32)
                scaled = readout * lax.rsqrt(jnp.mean(readout * readout, axis=-1, keepdims=True) + EPS)
                g = gv[at, vs].astype(f32)
                heads[t, pl.ds(r, 128), vs] = (scaled * gain * (g / (1.0 + jnp.exp(-g)))).astype(bf16)

    head_sends = []
    for i, dev in enumerate((L.xn, L.xo, L.core)):
        t = dev[1]
        finish(t)
        cp = remote(heads.at[t], hrecv.at[L.tp], h_s.at[i], h_r.at[i], dev)
        cp.start()
        head_sends.append(cp)
    finish(L.tp)
    hrecv[L.tp] = heads[L.tp]
    forward_inner(0, 3, 0)

    wo_from_x = remote(out_w, wo.at[L.xn[1]], wo_s.at[0], wo_r.at[0], L.xn)
    wo_from_x.wait_recv()
    relay = remote(wo.at[L.xn[1]], wo.at[L.xn[1]], wo_s.at[2], wo_r.at[2], L.core)
    relay.start()
    keep[1].wait()
    cross[1].wait_recv()
    for part in range(2):
        send_own(1, part)
        to_core(1, z, part).start()
    remote(out_w, wo.at[L.core[1]], wo_s.at[1], wo_r.at[1], L.core).wait_recv()
    remote(wo.at[L.xo[1]], wo.at[L.xo[1]], wo_s.at[2], wo_r.at[2], L.core).wait_recv()
    wo_own.wait()
    late[1].wait()
    for i, dev in enumerate((L.xn, L.xo, L.core)):
        remote(heads.at[dev[1]], hrecv.at[dev[1]], h_s.at[i], h_r.at[i], dev).wait_recv()
    forward_inner(0, 3, 1)

    square = jnp.zeros((rows, 1), f32)
    wide = min(512, width)
    for n in range(0, width, wide):
        cols = pl.ds(n, wide)
        acc = mid[:, cols].astype(f32)
        for t in range(n_tp):
            acc = acc + jnp.dot(hrecv[t], wo[t, :, cols], preferred_element_type=f32)
        m = acc.astype(bf16)
        mid[:, cols] = m
        m = m.astype(f32)
        square = square + jnp.sum(m * m, axis=-1, keepdims=True)
    norm = lax.rsqrt(square * (1.0 / width) + EPS)
    for n in range(0, width, wide):
        cols = pl.ds(n, wide)
        acts[0, :, cols] = (mid[:, cols].astype(f32) * norm * mix_gain[:, cols]).astype(bf16)

    halves = (pl.ds(0, half_rows), pl.ds(half_rows, half_rows))

    def act_copy(i):
        slot, part, dst, dev = [(0, 0, 1, L.xn), (0, 1, 1, L.xn), (0, 0, 2, L.yn), (0, 1, 2, L.yn), (1, 0, 3, L.yn), (2, 1, 3, L.xn)][i]
        return remote(acts.at[slot, halves[part], :], acts.at[dst, halves[part], :], a_s.at[i], a_r.at[i], dev)

    for i in (0, 3, 1, 2):
        act_copy(i).start()

    for s in range(1, nz):
        for part in range(2):
            @pl.when(edge)
            def _():
                arrive(0, s, part, False)

    def up_rows(i):
        def step(n, carry):
            core = n // (half // TILE)
            at = pl.ds(pl.multiple_of((n % (half // TILE)) * TILE, TILE), TILE)
            pre = jnp.dot(acts[i], up[core, :, at], preferred_element_type=f32)
            pre = jnp.maximum(pre, 0.0)
            hidden[i, :, pl.ds(pl.multiple_of(n * TILE, TILE), TILE)] = (pre * pre).astype(bf16)
            return carry

        lax.fori_loop(0, 2 * half // TILE, step, 0)

    keep[0].wait()
    for j in range(nz):
        for part in range(2):
            from_core(0, j, part).wait_recv()
    up_rows(0)
    forward_inner(1, 1, 0)
    forward_inner(1, 2, 0)
    act_copy(0).wait_recv()
    act_copy(4).start()
    act_copy(3).wait_recv()
    act_copy(5).start()
    act_copy(1).wait_recv()
    up_rows(1)
    forward_inner(1, 1, 1)
    forward_inner(1, 2, 1)
    act_copy(2).wait_recv()
    up_rows(2)
    forward_inner(1, 3, 0)
    act_copy(4).wait_recv()
    act_copy(5).wait_recv()
    up_rows(3)
    forward_inner(1, 3, 1)

    a, b = halves

    def columns(t):
        d = L.piece(t // 2) * 2 + t % 2
        return d, pl.ds(pl.multiple_of(d * slab, slab), slab)

    def part_copy(i, t):
        d, cols = columns(t)
        src, dst, dev = [
            (psend.at[2, a, cols], pass_y.at[:, cols], L.yn),
            (psend.at[2, b, cols], pass_x.at[:, cols], L.xn),
            (psend.at[0, b, cols], sum_x.at[b, cols], L.xn),
            (psend.at[1, a, cols], sum_y.at[a, cols], L.yn),
            (psend.at[0, a, cols], sum_x.at[a, cols], L.xn),
            (psend.at[1, b, cols], sum_y.at[b, cols], L.yn),
        ][i]
        return remote(src, dst, p_s.at[i, d], p_r.at[i, d], dev)

    def down_step(t, carry):
        @pl.when(t < np_)
        def _():
            s, part = t // 2, t % 2
            j = L.piece(s)

            @pl.when(jnp.logical_and(edge, t >= 2))
            def _():
                arrive(1, s, part, False)

            from_core(1, j, part).wait_recv()
            _, cols = columns(t)
            w0, w1 = place(1, 0, j, part), place(1, 1, j, part)

            def rows_of(i):
                return lax.dot_general(
                    hidden[i, :, :half], w0[...], NT, preferred_element_type=f32
                ) + lax.dot_general(hidden[i, :, half:], w1[...], NT, preferred_element_type=f32)

            psend[2, :, cols] = rows_of(3).astype(bf16)
            part_copy(0, t).start()
            part_copy(1, t).start()
            psend[0, :, cols] = rows_of(1).astype(bf16)
            part_copy(2, t).start()
            psend[1, :, cols] = rows_of(2).astype(bf16)
            part_copy(3, t).start()
            pown[:, cols] = rows_of(0)

        @pl.when(jnp.logical_and(t >= 1, t < np_ + 1))
        def _():
            u = t - 1
            _, cols = columns(u)
            part_copy(0, u).wait_recv()
            psend[0, a, cols] = (psend[0, a, cols].astype(f32) + pass_y[:, cols].astype(f32)).astype(bf16)
            part_copy(4, u).start()
            part_copy(1, u).wait_recv()
            psend[1, b, cols] = (psend[1, b, cols].astype(f32) + pass_x[:, cols].astype(f32)).astype(bf16)
            part_copy(5, u).start()

        @pl.when(t >= 2)
        def _():
            u = t - 2
            d, cols = columns(u)
            for i in (2, 3, 4, 5):
                part_copy(i, u).wait_recv()
            feed = pown[:, cols] + sum_x[:, cols].astype(f32) + sum_y[:, cols].astype(f32)
            outv[:, cols] = (mid[:, cols].astype(f32) + feed).astype(bf16)
            pltpu.make_async_copy(outv.at[:, cols], out.at[:, cols], o_s.at[d]).start()

        return carry

    lax.fori_loop(0, np_ + 2, down_step, 0)

    for k in range(2):
        cross[k].wait_send()
        for part in range(2):
            for side in range(2):
                @pl.when((z < nz - 1) if side else (z > 0))
                def _():
                    to_side(k, part, side).wait_send()
            for s in range(nz):
                j = L.piece(s)
                to_core(k, j, part).wait_send()
                if s:
                    @pl.when(inner)
                    def _():
                        onward(k, j, part).wait_send()
    for cp in [wo_x, wo_c, relay, swap, back] + head_sends + [act_copy(i) for i in range(6)]:
        cp.wait_send()
    for zz in range(1, nz):
        @pl.when(z < zz)
        def _():
            hand_on(zz).wait_send()
    for t in range(np_):
        for i in range(6):
            part_copy(i, t).wait_send()
        d, cols = columns(t)
        pltpu.make_async_copy(outv.at[:, cols], out.at[:, cols], o_s.at[d]).wait()


def fused(
    n_sp, n_tp, stream, query, key, value, gate, rates, head_gain, out_w, mix_gain, up_w, down_w
):
    f32, bf16 = jnp.float32, jnp.bfloat16
    rows, width = stream.shape
    n_heads = query.shape[1] // KEY_CHANNELS
    half = up_w.shape[1] // 2
    nz, np_ = n_sp // 2, n_sp
    K = KEY_CHANNELS
    V, D = pltpu.VMEM, pltpu.SemaphoreType.DMA
    hbm = pl.BlockSpec(memory_space=pltpu.HBM)
    vmem = pl.BlockSpec(memory_space=pltpu.VMEM)
    return pl.pallas_call(
        functools.partial(layer_kernel, n_sp, n_tp),
        out_shape=jax.ShapeDtypeStruct((rows, width), bf16),
        in_specs=[hbm] * 6 + [vmem] * 2 + [hbm] * 3,
        out_specs=hbm,
        scratch_shapes=[
            V((2, width, half), bf16), V((2, width, half), bf16), V((n_tp, out_w.shape[0], width), bf16),
            V(query.shape, bf16), V(key.shape, bf16), V(value.shape, bf16), V(gate.shape, bf16), V(rates.shape, f32),
            V(value.shape, f32), V(query.shape, bf16), V((n_heads, DV, K), f32), V((n_heads, 1, K), f32),
            V((n_heads, DV + 16, K), bf16), V((DV + 16, K), bf16), V((DV + 16, K), bf16), V((nz, DV + 16, K), bf16),
            V((DV, K), f32), V((DV, K), bf16), V((n_heads, DV, K), bf16),
            V((n_tp, rows, value.shape[1]), bf16), V((n_tp, rows, value.shape[1]), bf16),
            V((4, rows, width), bf16), V((4, rows, 2 * half), bf16), V((rows, width), bf16),
            V((3, rows, width), bf16), V((rows, width), f32), V((rows, width), bf16), V((rows, width), bf16),
            V((rows // 2, width), bf16), V((rows // 2, width), bf16), V((rows, width), bf16),
            D((9,)), D((2, 2, 2)), D((2, nz, 2)), D((2, nz, 2)), D((2,)), D((2,)), D((2, nz, 2)), D((2, nz, 2)),
            D((3,)), D((3,)), D((2,)), D((2,)), D((nz,)), D((nz,)), D((3,)), D((3,)), D((6,)), D((6,)),
            D((6, np_)), D((6, np_)), D((np_,)),
        ],
        compiler_params=pltpu.CompilerParams(
            collective_id=0, has_side_effects=True, vmem_limit_bytes=67_000_000
        ),
        name="layer",
    )(stream, query, key, value, gate, rates, head_gain.reshape(1, -1), mix_gain.reshape(1, -1), out_w, up_w, down_w)


def solution(mesh):
    placed = (
        P(("sp", "tp"), None),
        P("sp", "tp"),
        P("sp", "tp"),
        P("sp", "tp"),
        P("sp", "tp"),
        P("sp", "tp"),
        P(),
        P("tp", None),
        P(),
        P("sp", "tp"),
        P("sp", "tp"),
    )

    def body(*args):
        return local(mesh.shape["sp"], mesh.shape["tp"], *args)

    if mesh.shape["tp"] == 4 and mesh.shape["sp"] % 2 == 0:
        def whole(*args):
            return fused(mesh.shape["sp"], mesh.shape["tp"], *args)

        return jax.shard_map(whole, mesh=mesh, in_specs=placed, out_specs=P(("sp", "tp"), None), check_vma=False)
    return jax.shard_map(body, mesh=mesh, in_specs=placed, out_specs=P(("sp", "tp"), None), check_vma=False)
```

profile of v0, /device:TPU:0, one launch (start us, length us, event | category | flops | bytes accessed | tf_op | source)
XLA Modules:
  0.0 166.7 jit_solution(9137922459938936669)
XLA Ops:
  0.0 164.4 %layer.1 = bf16[256,2048]{1,0:T(8,128)(2,1)} custom-call(bf16[256,2048]{1,0:T(8,128)(2,1)} %stream.1, bf16[1024,256]{1,0:T(8,128)(2,1)} %query.1, bf16[1024,256]{1,0:T(8,128)(2,1)} %key.1, bf16[1024,512]{1,0:T(8,128)(2,1)} %value.1, bf16[1024,512]{1,0:T(8,128)(2,1)} %gate.1, f32[1024,256]{1,0:T(8,128)} %rates_in.1, f32[1,256]{1,0:T(1,128)} %bitcast.3, ...), custom_call_target="tpu_custom_call" | custom-call | tf_op jit(solution)/shard_map/layer/pallas_call | solution.py:680
  164.4 2.3 %copy.13 = bf16[256,2048]{1,0:T(8,128)(2,1)} copy(bf16[256,2048]{1,0:T(8,128)(2,1)} %layer.1) | data formatting | bytes 2097152
where the time goes:
time: 168 us; the launch traced here: 167 us
  Pallas kernels  164 us (98%)
  local copies, waits for them, and re-layouts  2.3 us (1%)
    pallas_call x1, Pallas kernels, fused(): pl.pallas_call(functools.partial(layer_kernel, n_sp, n_tp), out_shape=jax...  164 us

commit v1 on v0

--- a/solution.py
+++ b/solution.py
@@ -253,7 +253,8 @@
     return out
 
 
-TILE = 256
+UP_TILE = 512
+CUT = 2
 MESH = pl.DeviceIdType.MESH
 
 
@@ -288,8 +289,8 @@
 def layer_kernel(
     n_sp, n_tp, stream, query, key, value, gate, rates_in, head_gain, mix_gain, out_w, up_w, down_w, out,
     up, down, wo, qv, kv, vv, gv, ldv, own, qd, state, total, summ, peer, tsend, trecv, prefix, bsend, before,
-    heads, hrecv, acts, hidden, mid, psend, pown, sum_x, sum_y, pass_y, pass_x, outv,
-    ld_s, zown_s, zfwd_s, z_r, y_s, y_r, d_s, d_r, wo_s, wo_r, s_s, s_r, t_s, t_r, h_s, h_r, a_s, a_r, p_s, p_r, o_s,
+    heads, hrecv, acts, hidden, mid, psend, pown, sum_x, sum_y, pass_y, pass_x,
+    ld_s, zown_s, zfwd_s, z_r, y_s, y_r, d_s, d_r, wo_s, wo_r, s_s, s_r, t_s, t_r, h_s, h_r, a_s, a_r, p_s, p_r,
 ):
     f32, bf16 = jnp.float32, jnp.bfloat16
     L = Links(n_sp)
@@ -299,56 +300,64 @@
     n_heads = query.shape[1] // KEY_CHANNELS
     slab, half = up_w.shape[0], up_w.shape[1] // 2
     half_rows = rows // 2
-    np_ = 2 * nz
+    fine = slab // CUT
 
     loads = [(query, qv), (key, kv), (value, vv), (rates_in, ldv)]
     first = [pltpu.make_async_copy(a, b, ld_s.at[i]) for i, (a, b) in enumerate(loads)]
     for cp in first:
         cp.start()
     barrier = pltpu.get_barrier_semaphore()
-    partners = [L.core, L.xn, L.xo, L.yn] + [L.at_z((z + k) % nz) for k in range(1, nz)]
+    partners = [L.core, L.xn, L.xo, L.yn]
     for dev in partners:
         pl.semaphore_signal(barrier, inc=1, device_id=dev, device_id_type=MESH)
-    pl.semaphore_wait(barrier, len(partners))
-
-    bufs, source = (up, down), (up_w, down_w)
-
-    def place(kind, core, j, part):
-        row = j * 2 + (part if kind else (y + part) % 2)
-        return bufs[kind].at[core, pl.ds(pl.multiple_of(row * slab, slab), slab), :]
-
-    def halfcols(kind, h):
-        return source[kind].at[:, pl.ds(pl.multiple_of(h * half, half), half)]
-
-    def own_rows(kind, yy):
-        return bufs[kind].at[c, pl.ds(pl.multiple_of((z * 2 + yy) * slab, slab), slab), :]
-
-    keep = [pltpu.make_async_copy(halfcols(k, y), own_rows(k, y), ld_s.at[6 + k]) for k in range(2)]
-    cross = [
-        remote(halfcols(k, 1 - y), own_rows(k, y), y_s.at[k], y_r.at[k], L.yn) for k in range(2)
-    ]
-
-    def to_side(kind, part, side):
-        to = z + (1 if side else -1)
-        src = halfcols(0, y) if (kind, part) == (0, 0) else place(kind, c, z, part)
-        return remote(src, place(kind, c, z, part), zown_s.at[kind, part, side], z_r.at[kind, z, part], L.at_z((to + nz) % nz))
-
-    def to_core(kind, j, part, from_hbm=False):
+    for has, to in ((z > 0, z - 1), (z < nz - 1, z + 1)):
+        @pl.when(has)
+        def _():
+            pl.semaphore_signal(barrier, inc=1, device_id=L.at_z((to + nz) % nz), device_id_type=MESH)
+
+    ends = jnp.where(z > 0, 1, 0) + jnp.where(z < nz - 1, 1, 0)
+    pl.semaphore_wait(barrier, len(partners) + ends)
+
+    bufs, source, cuts = (up, down), (up_w, down_w), (1, CUT)
+
+    def place(kind, core, j, part, n=1):
+        size = slab // cuts[kind]
+        return bufs[kind].at[
+            pl.ds(pl.multiple_of((j * 2 * cuts[kind] + part) * size, size), n * size),
+            pl.ds(pl.multiple_of(core * half, half), half),
+        ]
+
+    def halfcols(kind, h, cut=None):
+        size = slab // cuts[kind]
+        return source[kind].at[pl.ds(0, slab) if cut is None else pl.ds(cut * size, size), pl.ds(pl.multiple_of(h * half, half), half)]
+
+    def whole_part(kind, yy):
+        return place(kind, c, z, yy * cuts[kind], cuts[kind])
+
+    keep = [pltpu.make_async_copy(halfcols(k, y), whole_part(k, y), ld_s.at[6 + k]) for k in range(2)]
+    cross = [remote(halfcols(k, 1 - y), whole_part(k, y), y_s.at[k], y_r.at[k], L.yn) for k in range(2)]
+
+    def to_side(kind, far, cut, side):
+        part = (1 - y if far else y) * cuts[kind] + cut
+        src = place(kind, c, z, part) if far else halfcols(kind, y, cut)
+        to = L.at_z((z + (1 if side else -1) + nz) % nz)
+        return remote(src, place(kind, c, z, part), zown_s.at[kind, far, cut, side], z_r.at[kind, z, part], to)
+
+    def to_core(kind, j, part, cut=None):
         dst = place(kind, c, j, part)
-        return remote(halfcols(kind, y) if from_hbm else dst, dst, d_s.at[kind, j, part], d_r.at[kind, j, part], L.core)
-
-    def send_own(kind, part, sides=(0, 1)):
+        src = dst if cut is None else halfcols(kind, y, cut)
+        return remote(src, dst, d_s.at[kind, j, part], d_r.at[kind, j, part], L.core)
+
+    def send_own(kind, far, sides=(0, 1)):
         for side in sides:
             @pl.when((z < nz - 1) if side else (z > 0))
             def _():
-                to_side(kind, part, side).start()
-
-    def open_part(part):
-        if part == 0:
-            keep[0].start()
-        else:
-            cross[0].wait_recv()
-        to_core(0, z, part, part == 0).start()
+                for cut in range(cuts[kind]):
+                    to_side(kind, far, cut, side).start()
+
+    def share_own(kind, far):
+        for cut in range(cuts[kind]):
+            to_core(kind, z, (1 - y if far else y) * cuts[kind] + cut, None if far else cut).start()
 
     def onward(kind, j, part):
         to = jnp.where(j < z, z + 1, z - 1)
@@ -371,20 +380,38 @@
         def _():
             arrive(kind, s, part, True)
 
+    def arrive_edge(kind, s, part):
+        @pl.when(edge)
+        def _():
+            arrive(kind, s, part, False)
+
     def from_core(kind, j, part):
         dst = place(kind, 1 - c, j, part)
         return remote(dst, dst, d_s.at[kind, j, part], d_r.at[kind, j, part], L.core)
 
-    cross[0].start()
     send_own(0, 0)
+    send_own(1, 0, (0,))
+    wo_half, wo_quarter = out_w.shape[0] // 2, out_w.shape[0] // 4
+
+    def wo_rows(k):
+        return pl.ds(0, wo_half) if k is None else pl.ds(pl.multiple_of(wo_half + k * wo_quarter, wo_quarter), wo_quarter)
+
     wo_own = pltpu.make_async_copy(out_w, wo.at[L.tp], ld_s.at[4])
-    wo_x = remote(out_w, wo.at[L.tp], wo_s.at[0], wo_r.at[0], L.xn)
     wo_c = remote(out_w, wo.at[L.tp], wo_s.at[1], wo_r.at[1], L.core)
-    wo_x.start()
+    wo_b = remote(out_w.at[wo_rows(y), :], wo.at[L.tp, wo_rows(y), :], wo_s.at[3], wo_r.at[3], L.xn)
+    wo_a = remote(out_w.at[wo_rows(None), :], wo.at[L.tp, wo_rows(None), :], wo_s.at[0], wo_r.at[0], L.xn)
+
+    def wo_pass(k):
+        ref = wo.at[L.xn[1], wo_rows(k), :]
+        return remote(ref, ref, wo_s.at[4], wo_r.at[4], L.yn)
+
+    wo_b.start()
+    wo_a.start()
     wo_c.start()
     wo_own.start()
-    open_part(0)
-    keep[1].start()
+    for k in range(2):
+        keep[k].start()
+        share_own(k, 0)
     late = [pltpu.make_async_copy(gate, gv, ld_s.at[5]), pltpu.make_async_copy(stream, mid, ld_s.at[8])]
     for cp in late:
         cp.start()
@@ -416,51 +443,65 @@
             qd[at, ks] = (q.astype(f32) * (jnp.exp(tot) * scale)).astype(bf16)
         return carry
 
-    lax.fori_loop(0, span // BLOCK, block, 0, unroll=2)
+    lax.fori_loop(0, span // BLOCK, block, 0, unroll=4)
     for h in range(n_heads):
         summ[h, :DV, :] = state[h].astype(bf16)
         summ[h, DV:, :] = jnp.broadcast_to(jnp.exp(total[h]), (16, KEY_CHANNELS)).astype(bf16)
 
     swap = remote(summ.at[1 - y], peer, s_s.at[0], s_r.at[0], L.yn)
     swap.start()
-    open_part(1)
-    send_own(0, 1)
+    cross[0].start()
     swap.wait_recv()
     mine, other = summ[y].astype(f32), peer[...].astype(f32)
     is0 = y == 0
     early, late_ = jnp.where(is0, mine, other), jnp.where(is0, other, mine)
     dec = late_[DV : DV + 1]
-    tsend[:DV, :] = (dec * early[:DV] + late_[:DV]).astype(bf16)
-    tsend[DV:, :] = (dec * early[DV:]).astype(bf16)
-
-    def hand_on(zz):
-        return remote(tsend, trecv.at[z], t_s.at[zz], t_r.at[z], L.at_z(zz))
-
-    for zz in range(1, nz):
-        @pl.when(z < zz)
-        def _():
-            hand_on(zz).start()
-    forward_inner(0, 1, 0)
-    forward_inner(0, 2, 0)
+    here = dec * early[:DV] + late_[:DV]
+    onto_here = dec * early[DV : DV + 1]
+
+    def hand_on(to):
+        return remote(tsend, trecv, t_s.at[0], t_r.at[0], L.at_z((to + nz) % nz))
+
+    @pl.when(z == nz - 2)
+    def _():
+        to_side(1, 0, 0, 1).start()
+
     prefix[...] = jnp.zeros_like(prefix)
-    for j in range(nz - 1):
-        @pl.when(j < z)
-        def _():
-            remote(tsend, trecv.at[j], t_s.at[j], t_r.at[j], L.at_z(j)).wait_recv()
-            got = trecv[j].astype(f32)
-            prefix[...] = got[DV : DV + 1] * prefix[...] + got[:DV]
+
+    @pl.when(z > 0)
+    def _():
+        hand_on(z).wait_recv()
+        prefix[...] = trecv[...].astype(f32)
+
     whole = prefix[...]
+
+    @pl.when(z < nz - 1)
+    def _():
+        tsend[...] = (onto_here * whole + here).astype(bf16)
+        hand_on(z + 1).start()
+        for cut in range(1, CUT):
+            to_side(1, 0, cut, 1).start()
+
+    @pl.when(z < nz - 2)
+    def _():
+        to_side(1, 0, 0, 1).start()
+
     first_y = jnp.where(is0, mine, other)
     onto = first_y[DV : DV + 1] * whole + first_y[:DV]
     bsend[...] = jnp.where(is0, onto, whole).astype(bf16)
     before[y] = jnp.where(is0, whole, onto).astype(bf16)
     back = remote(bsend, before.at[y], s_s.at[1], s_r.at[1], L.yn)
     back.start()
-    forward_inner(0, 1, 1)
-    forward_inner(0, 2, 1)
+    wo_from_b = remote(out_w.at[wo_rows(y), :], wo.at[L.xn[1], wo_rows(y), :], wo_s.at[3], wo_r.at[3], L.xn)
+    wo_from_b.wait_recv()
+    wo_pass(y).start()
+    cross[1].start()
+    cross[0].wait_recv()
+    send_own(0, 1)
+    share_own(0, 1)
+    forward_inner(0, 1, y)
+    forward_inner(0, 2, y)
     remote(bsend, before.at[1 - y], s_s.at[1], s_r.at[1], L.yn).wait_recv()
-    cross[1].start()
-
     late[0].wait()
     gain = head_gain[...]
 
@@ -483,24 +524,22 @@
         head_sends.append(cp)
     finish(L.tp)
     hrecv[L.tp] = heads[L.tp]
-    forward_inner(0, 3, 0)
-
-    wo_from_x = remote(out_w, wo.at[L.xn[1]], wo_s.at[0], wo_r.at[0], L.xn)
-    wo_from_x.wait_recv()
+    forward_inner(0, 1, 1 - y)
+    forward_inner(0, 2, 1 - y)
+
+    remote(out_w.at[wo_rows(None), :], wo.at[L.xn[1], wo_rows(None), :], wo_s.at[0], wo_r.at[0], L.xn).wait_recv()
+    wo_pass(1 - y).wait_recv()
     relay = remote(wo.at[L.xn[1]], wo.at[L.xn[1]], wo_s.at[2], wo_r.at[2], L.core)
     relay.start()
-    keep[1].wait()
-    cross[1].wait_recv()
-    for part in range(2):
-        send_own(1, part)
-        to_core(1, z, part).start()
     remote(out_w, wo.at[L.core[1]], wo_s.at[1], wo_r.at[1], L.core).wait_recv()
     remote(wo.at[L.xo[1]], wo.at[L.xo[1]], wo_s.at[2], wo_r.at[2], L.core).wait_recv()
     wo_own.wait()
     late[1].wait()
+    forward_inner(0, 3, y)
+    arrive_edge(0, 1, y)
+    arrive_edge(0, 1, 1 - y)
     for i, dev in enumerate((L.xn, L.xo, L.core)):
         remote(heads.at[dev[1]], hrecv.at[dev[1]], h_s.at[i], h_r.at[i], dev).wait_recv()
-    forward_inner(0, 3, 1)
 
     square = jnp.zeros((rows, 1), f32)
     wide = min(512, width)
@@ -516,65 +555,62 @@
     norm = lax.rsqrt(square * (1.0 / width) + EPS)
     for n in range(0, width, wide):
         cols = pl.ds(n, wide)
-        acts[0, :, cols] = (mid[:, cols].astype(f32) * norm * mix_gain[:, cols]).astype(bf16)
-
-    halves = (pl.ds(0, half_rows), pl.ds(half_rows, half_rows))
+        acts[:rows, cols] = (mid[:, cols].astype(f32) * norm * mix_gain[:, cols]).astype(bf16)
+
+    a, b = pl.ds(0, half_rows), pl.ds(half_rows, half_rows)
 
     def act_copy(i):
         slot, part, dst, dev = [(0, 0, 1, L.xn), (0, 1, 1, L.xn), (0, 0, 2, L.yn), (0, 1, 2, L.yn), (1, 0, 3, L.yn), (2, 1, 3, L.xn)][i]
-        return remote(acts.at[slot, halves[part], :], acts.at[dst, halves[part], :], a_s.at[i], a_r.at[i], dev)
+        src = acts.at[pl.ds(slot * rows + part * half_rows, half_rows), :]
+        return remote(src, acts.at[pl.ds(dst * rows + part * half_rows, half_rows), :], a_s.at[i], a_r.at[i], dev)
 
     for i in (0, 3, 1, 2):
         act_copy(i).start()
-
-    for s in range(1, nz):
-        for part in range(2):
-            @pl.when(edge)
-            def _():
-                arrive(0, s, part, False)
-
-    def up_rows(i):
-        def step(n, carry):
-            core = n // (half // TILE)
-            at = pl.ds(pl.multiple_of((n % (half // TILE)) * TILE, TILE), TILE)
-            pre = jnp.dot(acts[i], up[core, :, at], preferred_element_type=f32)
-            pre = jnp.maximum(pre, 0.0)
-            hidden[i, :, pl.ds(pl.multiple_of(n * TILE, TILE), TILE)] = (pre * pre).astype(bf16)
-            return carry
-
-        lax.fori_loop(0, 2 * half // TILE, step, 0)
-
+    forward_inner(0, 3, 1 - y)
+    cross[1].wait_recv()
+    send_own(1, 1)
+    share_own(1, 1)
+    act_copy(0).wait_recv()
+    act_copy(4).start()
+    act_copy(3).wait_recv()
+    act_copy(5).start()
+    for s in (1, 2):
+        for part in range(2 * CUT):
+            forward_inner(1, s, part)
+    arrive_edge(0, 2, y)
+    arrive_edge(0, 2, 1 - y)
+    for i in (1, 2, 4, 5):
+        act_copy(i).wait_recv()
+    for part in range(CUT):
+        forward_inner(1, 3, part)
+
+    arrive_edge(0, 3, y)
+    arrive_edge(0, 3, 1 - y)
     keep[0].wait()
     for j in range(nz):
         for part in range(2):
             from_core(0, j, part).wait_recv()
-    up_rows(0)
-    forward_inner(1, 1, 0)
-    forward_inner(1, 2, 0)
-    act_copy(0).wait_recv()
-    act_copy(4).start()
-    act_copy(3).wait_recv()
-    act_copy(5).start()
-    act_copy(1).wait_recv()
-    up_rows(1)
-    forward_inner(1, 1, 1)
-    forward_inner(1, 2, 1)
-    act_copy(2).wait_recv()
-    up_rows(2)
-    forward_inner(1, 3, 0)
-    act_copy(4).wait_recv()
-    act_copy(5).wait_recv()
-    up_rows(3)
-    forward_inner(1, 3, 1)
-
-    a, b = halves
-
-    def columns(t):
-        d = L.piece(t // 2) * 2 + t % 2
-        return d, pl.ds(pl.multiple_of(d * slab, slab), slab)
-
-    def part_copy(i, t):
-        d, cols = columns(t)
+
+    def up_step(n, carry):
+        at = pl.ds(pl.multiple_of(n * UP_TILE, UP_TILE), UP_TILE)
+        pre = jnp.maximum(jnp.dot(acts[...], up[:, at], preferred_element_type=f32), 0.0)
+        hidden[:, at] = (pre * pre).astype(bf16)
+        return carry
+
+    lax.fori_loop(0, 2 * half // UP_TILE, up_step, 0)
+    for part in range(CUT, 2 * CUT):
+        forward_inner(1, 3, part)
+    keep[1].wait()
+
+    steps = 2 * nz * CUT
+    final = steps - CUT
+
+    def columns(u, n=1):
+        d = (L.piece(u // (2 * CUT)) * 2 * CUT + u % (2 * CUT)) * fine
+        return pl.ds(pl.multiple_of(d, fine), n * fine)
+
+    def part_copy(i, u):
+        cols = columns(u)
         src, dst, dev = [
             (psend.at[2, a, cols], pass_y.at[:, cols], L.yn),
             (psend.at[2, b, cols], pass_x.at[:, cols], L.xn),
@@ -583,68 +619,73 @@
             (psend.at[0, a, cols], sum_x.at[a, cols], L.xn),
             (psend.at[1, b, cols], sum_y.at[b, cols], L.yn),
         ][i]
-        return remote(src, dst, p_s.at[i, d], p_r.at[i, d], dev)
-
-    def down_step(t, carry):
-        @pl.when(t < np_)
+        return remote(src, dst, p_s.at[i, u], p_r.at[i, u], dev)
+
+    def terms_of(u, n):
+        s = u // (2 * CUT)
+
+        @pl.when(jnp.logical_and(edge, s > 0))
         def _():
-            s, part = t // 2, t % 2
-            j = L.piece(s)
-
-            @pl.when(jnp.logical_and(edge, t >= 2))
-            def _():
-                arrive(1, s, part, False)
-
-            from_core(1, j, part).wait_recv()
-            _, cols = columns(t)
-            w0, w1 = place(1, 0, j, part), place(1, 1, j, part)
-
-            def rows_of(i):
-                return lax.dot_general(
-                    hidden[i, :, :half], w0[...], NT, preferred_element_type=f32
-                ) + lax.dot_general(hidden[i, :, half:], w1[...], NT, preferred_element_type=f32)
-
-            psend[2, :, cols] = rows_of(3).astype(bf16)
-            part_copy(0, t).start()
-            part_copy(1, t).start()
-            psend[0, :, cols] = rows_of(1).astype(bf16)
-            part_copy(2, t).start()
-            psend[1, :, cols] = rows_of(2).astype(bf16)
-            part_copy(3, t).start()
-            pown[:, cols] = rows_of(0)
-
-        @pl.when(jnp.logical_and(t >= 1, t < np_ + 1))
+            for k in range(n):
+                arrive(1, s, u % (2 * CUT) + k, False)
+
+        for k in range(n):
+            from_core(1, L.piece(s), u % (2 * CUT) + k).wait_recv()
+        cols = columns(u, n)
+        terms = lax.dot_general(hidden[...], down[cols, :], NT, preferred_element_type=f32)
+        pown[:, cols] = terms[:rows]
+        for i in range(3):
+            psend[i, :, cols] = terms[(i + 1) * rows : (i + 2) * rows].astype(bf16)
+        for i in range(4):
+            for k in range(n):
+                part_copy(i, u + k).start()
+
+    def pass_on(u):
+        cols = columns(u)
+        part_copy(0, u).wait_recv()
+        psend[0, a, cols] = (psend[0, a, cols].astype(f32) + pass_y[:, cols].astype(f32)).astype(bf16)
+        part_copy(4, u).start()
+        part_copy(1, u).wait_recv()
+        psend[1, b, cols] = (psend[1, b, cols].astype(f32) + pass_x[:, cols].astype(f32)).astype(bf16)
+        part_copy(5, u).start()
+
+    def close(u):
+        cols = columns(u)
+        for i in (2, 3, 4, 5):
+            part_copy(i, u).wait_recv()
+        feed = pown[:, cols] + sum_x[:, cols].astype(f32) + sum_y[:, cols].astype(f32)
+        out[:, cols] = (mid[:, cols].astype(f32) + feed).astype(bf16)
+
+    def down_step(u, carry):
+        @pl.when(jnp.logical_and(u < final, u % CUT == 0))
         def _():
-            u = t - 1
-            _, cols = columns(u)
-            part_copy(0, u).wait_recv()
-            psend[0, a, cols] = (psend[0, a, cols].astype(f32) + pass_y[:, cols].astype(f32)).astype(bf16)
-            part_copy(4, u).start()
-            part_copy(1, u).wait_recv()
-            psend[1, b, cols] = (psend[1, b, cols].astype(f32) + pass_x[:, cols].astype(f32)).astype(bf16)
-            part_copy(5, u).start()
-
-        @pl.when(t >= 2)
+            terms_of(u, CUT)
+
+        @pl.when(jnp.logical_and(u >= final, u < steps))
         def _():
-            u = t - 2
-            d, cols = columns(u)
-            for i in (2, 3, 4, 5):
-                part_copy(i, u).wait_recv()
-            feed = pown[:, cols] + sum_x[:, cols].astype(f32) + sum_y[:, cols].astype(f32)
-            outv[:, cols] = (mid[:, cols].astype(f32) + feed).astype(bf16)
-            pltpu.make_async_copy(outv.at[:, cols], out.at[:, cols], o_s.at[d]).start()
+            terms_of(u, 1)
+
+        @pl.when(jnp.logical_and(u >= CUT, u < steps + CUT))
+        def _():
+            pass_on(u - CUT)
+
+        @pl.when(u >= 2 * CUT)
+        def _():
+            close(u - 2 * CUT)
 
         return carry
 
-    lax.fori_loop(0, np_ + 2, down_step, 0)
+    lax.fori_loop(0, steps + 2 * CUT, down_step, 0)
 
     for k in range(2):
         cross[k].wait_send()
-        for part in range(2):
+        for far in range(2):
             for side in range(2):
                 @pl.when((z < nz - 1) if side else (z > 0))
                 def _():
-                    to_side(k, part, side).wait_send()
+                    for cut in range(cuts[k]):
+                        to_side(k, far, cut, side).wait_send()
+        for part in range(2 * cuts[k]):
             for s in range(nz):
                 j = L.piece(s)
                 to_core(k, j, part).wait_send()
@@ -652,17 +693,16 @@
                     @pl.when(inner)
                     def _():
                         onward(k, j, part).wait_send()
-    for cp in [wo_x, wo_c, relay, swap, back] + head_sends + [act_copy(i) for i in range(6)]:
+    for cp in [wo_a, wo_b, wo_c, wo_pass(y), relay, swap, back] + head_sends + [act_copy(i) for i in range(6)]:
         cp.wait_send()
-    for zz in range(1, nz):
-        @pl.when(z < zz)
-        def _():
-            hand_on(zz).wait_send()
-    for t in range(np_):
+
+    @pl.when(z < nz - 1)
+    def _():
+        hand_on(z + 1).wait_send()
+
+    for u in range(steps):
         for i in range(6):
-            part_copy(i, t).wait_send()
-        d, cols = columns(t)
-        pltpu.make_async_copy(outv.at[:, cols], out.at[:, cols], o_s.at[d]).wait()
+            part_copy(i, u).wait_send()
 
 
 def fused(
@@ -672,32 +712,33 @@
     rows, width = stream.shape
     n_heads = query.shape[1] // KEY_CHANNELS
     half = up_w.shape[1] // 2
-    nz, np_ = n_sp // 2, n_sp
+    nz, np_ = n_sp // 2, n_sp * CUT
     K = KEY_CHANNELS
     V, D = pltpu.VMEM, pltpu.SemaphoreType.DMA
     hbm = pl.BlockSpec(memory_space=pltpu.HBM)
     vmem = pl.BlockSpec(memory_space=pltpu.VMEM)
     return pl.pallas_call(
         functools.partial(layer_kernel, n_sp, n_tp),
-        out_shape=jax.ShapeDtypeStruct((rows, width), bf16),
+        out_shape=pltpu.VMEM((rows, width), bf16),
         in_specs=[hbm] * 6 + [vmem] * 2 + [hbm] * 3,
-        out_specs=hbm,
+        out_specs=vmem,
         scratch_shapes=[
-            V((2, width, half), bf16), V((2, width, half), bf16), V((n_tp, out_w.shape[0], width), bf16),
+            V((width, 2 * half), bf16), V((width, 2 * half), bf16), V((n_tp, out_w.shape[0], width), bf16),
             V(query.shape, bf16), V(key.shape, bf16), V(value.shape, bf16), V(gate.shape, bf16), V(rates.shape, f32),
             V(value.shape, f32), V(query.shape, bf16), V((n_heads, DV, K), f32), V((n_heads, 1, K), f32),
-            V((n_heads, DV + 16, K), bf16), V((DV + 16, K), bf16), V((DV + 16, K), bf16), V((nz, DV + 16, K), bf16),
+            V((n_heads, DV + 16, K), bf16), V((DV + 16, K), bf16), V((DV, K), bf16), V((DV, K), bf16),
             V((DV, K), f32), V((DV, K), bf16), V((n_heads, DV, K), bf16),
             V((n_tp, rows, value.shape[1]), bf16), V((n_tp, rows, value.shape[1]), bf16),
-            V((4, rows, width), bf16), V((4, rows, 2 * half), bf16), V((rows, width), bf16),
+            V((4 * rows, width), bf16), V((4 * rows, 2 * half), bf16), V((rows, width), bf16),
             V((3, rows, width), bf16), V((rows, width), f32), V((rows, width), bf16), V((rows, width), bf16),
-            V((rows // 2, width), bf16), V((rows // 2, width), bf16), V((rows, width), bf16),
-            D((9,)), D((2, 2, 2)), D((2, nz, 2)), D((2, nz, 2)), D((2,)), D((2,)), D((2, nz, 2)), D((2, nz, 2)),
-            D((3,)), D((3,)), D((2,)), D((2,)), D((nz,)), D((nz,)), D((3,)), D((3,)), D((6,)), D((6,)),
-            D((6, np_)), D((6, np_)), D((np_,)),
+            V((rows // 2, width), bf16), V((rows // 2, width), bf16),
+            D((9,)), D((2, 2, CUT, 2)), D((2, nz, 2 * CUT)), D((2, nz, 2 * CUT)), D((2,)), D((2,)), D((2, nz, 2 * CUT)),
+            D((2, nz, 2 * CUT)),
+            D((5,)), D((5,)), D((2,)), D((2,)), D((1,)), D((1,)), D((3,)), D((3,)), D((6,)), D((6,)),
+            D((6, np_)), D((6, np_)),
         ],
         compiler_params=pltpu.CompilerParams(
-            collective_id=0, has_side_effects=True, vmem_limit_bytes=67_000_000
+            collective_id=0, has_side_effects=True, vmem_limit_bytes=58_000_000
         ),
         name="layer",
     )(stream, query, key, value, gate, rates, head_gain.reshape(1, -1), mix_gain.reshape(1, -1), out_w, up_w, down_w)

time: 168 us -> 154 us (0.917)
  Pallas kernels: 164 us -> 153 us
    pallas_call x1, Pallas kernels: 164 us -> 153 us  [fused(): pl.pallas_call(functools.partial(layer_kernel, n_sp, n_tp), out_shape=plt...]
where the time goes in v1:
time: 154 us
  Pallas kernels  153 us (99%)
    pallas_call x1, Pallas kernels, fused(): pl.pallas_call(functools.partial(layer_kernel, n_sp, n_tp), out_shape=plt...  153 us

profile of v1, /device:TPU:0, one launch (start us, length us, event | category | flops | bytes accessed | tf_op | source)
XLA Modules:
  0.0 153.9 jit_solution(1702903583000278318)
XLA Ops:
  0.0 153.0 %layer.1 = bf16[256,2048]{1,0:T(8,128)(2,1)S(1)} custom-call(bf16[256,2048]{1,0:T(8,128)(2,1)} %stream.1, bf16[1024,256]{1,0:T(8,128)(2,1)} %query.1, bf16[1024,256]{1,0:T(8,128)(2,1)} %key.1, bf16[1024,512]{1,0:T(8,128)(2,1)} %value.1, bf16[1024,512]{1,0:T(8,128)(2,1)} %gate.1, f32[1024,256]{1,0:T(8,128)} %rates_in.1, f32[1,256]{1,0:T(1,128)} %bitcast.3, ...), custom_call_target="tpu_custom_call" | custom-call | tf_op jit(solution)/shard_map/layer/pallas_call | solution.py:720
  153.0 1.0 copy.13

commit v2 on v1

--- a/solution.py
+++ b/solution.py
@@ -290,7 +290,8 @@
     n_sp, n_tp, stream, query, key, value, gate, rates_in, head_gain, mix_gain, out_w, up_w, down_w, out,
     up, down, wo, qv, kv, vv, gv, ldv, own, qd, state, total, summ, peer, tsend, trecv, prefix, bsend, before,
     heads, hrecv, acts, hidden, mid, psend, pown, sum_x, sum_y, pass_y, pass_x,
-    ld_s, zown_s, zfwd_s, z_r, y_s, y_r, d_s, d_r, wo_s, wo_r, s_s, s_r, t_s, t_r, h_s, h_r, a_s, a_r, p_s, p_r,
+    gain_h, gain_m, ld_s, zown_s, zfwd_s, z_r, y_s, y_r, d_s, du_r, dd_r, wo_s, wo_r, s_s, s_r, t_s, t_r, h_s, h_r, a_s, a_r,
+    p_s, p_r,
 ):
     f32, bf16 = jnp.float32, jnp.bfloat16
     L = Links(n_sp)
@@ -302,10 +303,6 @@
     half_rows = rows // 2
     fine = slab // CUT
 
-    loads = [(query, qv), (key, kv), (value, vv), (rates_in, ldv)]
-    first = [pltpu.make_async_copy(a, b, ld_s.at[i]) for i, (a, b) in enumerate(loads)]
-    for cp in first:
-        cp.start()
     barrier = pltpu.get_barrier_semaphore()
     partners = [L.core, L.xn, L.xo, L.yn]
     for dev in partners:
@@ -315,6 +312,10 @@
         def _():
             pl.semaphore_signal(barrier, inc=1, device_id=L.at_z((to + nz) % nz), device_id_type=MESH)
 
+    loads = [(query, qv), (key, kv), (value, vv), (rates_in, ldv)]
+    first = [pltpu.make_async_copy(a, b, ld_s.at[i]) for i, (a, b) in enumerate(loads)]
+    for cp in first:
+        cp.start()
     ends = jnp.where(z > 0, 1, 0) + jnp.where(z < nz - 1, 1, 0)
     pl.semaphore_wait(barrier, len(partners) + ends)
 
@@ -335,18 +336,29 @@
         return place(kind, c, z, yy * cuts[kind], cuts[kind])
 
     keep = [pltpu.make_async_copy(halfcols(k, y), whole_part(k, y), ld_s.at[6 + k]) for k in range(2)]
-    cross = [remote(halfcols(k, 1 - y), whole_part(k, y), y_s.at[k], y_r.at[k], L.yn) for k in range(2)]
+    cross = [remote(halfcols(k, 1 - y), whole_part(k, y), y_s.at[0], y_r.at[k], L.yn) for k in range(2)]
+
+    def z_slot(kind, part):
+        return part + 2 * kind
 
     def to_side(kind, far, cut, side):
         part = (1 - y if far else y) * cuts[kind] + cut
         src = place(kind, c, z, part) if far else halfcols(kind, y, cut)
         to = L.at_z((z + (1 if side else -1) + nz) % nz)
-        return remote(src, place(kind, c, z, part), zown_s.at[kind, far, cut, side], z_r.at[kind, z, part], to)
-
-    def to_core(kind, j, part, cut=None):
-        dst = place(kind, c, j, part)
+        return remote(src, place(kind, c, z, part), zown_s.at[side], z_r.at[z, z_slot(kind, part)], to)
+
+    final = (2 * nz - 1) * CUT
+
+    def core_r(kind, s, part):
+        if kind == 0:
+            return du_r.at[0]
+        u = s * 2 * CUT + part
+        return dd_r.at[jnp.where(u < final, u // CUT, final // CUT + u - final)]
+
+    def to_core(kind, s, part, cut=None):
+        dst = place(kind, c, L.piece(s), part)
         src = dst if cut is None else halfcols(kind, y, cut)
-        return remote(src, dst, d_s.at[kind, j, part], d_r.at[kind, j, part], L.core)
+        return remote(src, dst, d_s.at[kind], core_r(kind, s, part), L.core)
 
     def send_own(kind, far, sides=(0, 1)):
         for side in sides:
@@ -357,12 +369,12 @@
 
     def share_own(kind, far):
         for cut in range(cuts[kind]):
-            to_core(kind, z, (1 - y if far else y) * cuts[kind] + cut, None if far else cut).start()
+            to_core(kind, 0, (1 - y if far else y) * cuts[kind] + cut, None if far else cut).start()
 
     def onward(kind, j, part):
         to = jnp.where(j < z, z + 1, z - 1)
         dst = place(kind, c, j, part)
-        return remote(dst, dst, zfwd_s.at[kind, j, part], z_r.at[kind, j, part], L.at_z((to + nz) % nz))
+        return remote(dst, dst, zfwd_s.at[kind], z_r.at[j, z_slot(kind, part)], L.at_z((to + nz) % nz))
 
     inner = jnp.logical_and(z > 0, z < nz - 1)
     edge = jnp.logical_or(z == 0, z == nz - 1)
@@ -373,7 +385,7 @@
         cp.wait_recv()
         if forward:
             cp.start()
-        to_core(kind, j, part).start()
+        to_core(kind, s, part).start()
 
     def forward_inner(kind, s, part):
         @pl.when(inner)
@@ -384,10 +396,6 @@
         @pl.when(edge)
         def _():
             arrive(kind, s, part, False)
-
-    def from_core(kind, j, part):
-        dst = place(kind, 1 - c, j, part)
-        return remote(dst, dst, d_s.at[kind, j, part], d_r.at[kind, j, part], L.core)
 
     send_own(0, 0)
     send_own(1, 0, (0,))
@@ -397,13 +405,13 @@
         return pl.ds(0, wo_half) if k is None else pl.ds(pl.multiple_of(wo_half + k * wo_quarter, wo_quarter), wo_quarter)
 
     wo_own = pltpu.make_async_copy(out_w, wo.at[L.tp], ld_s.at[4])
-    wo_c = remote(out_w, wo.at[L.tp], wo_s.at[1], wo_r.at[1], L.core)
-    wo_b = remote(out_w.at[wo_rows(y), :], wo.at[L.tp, wo_rows(y), :], wo_s.at[3], wo_r.at[3], L.xn)
+    wo_c = remote(out_w, wo.at[L.tp], wo_s.at[0], wo_r.at[1], L.core)
+    wo_b = remote(out_w.at[wo_rows(y), :], wo.at[L.tp, wo_rows(y), :], wo_s.at[0], wo_r.at[3], L.xn)
     wo_a = remote(out_w.at[wo_rows(None), :], wo.at[L.tp, wo_rows(None), :], wo_s.at[0], wo_r.at[0], L.xn)
 
     def wo_pass(k):
         ref = wo.at[L.xn[1], wo_rows(k), :]
-        return remote(ref, ref, wo_s.at[4], wo_r.at[4], L.yn)
+        return remote(ref, ref, wo_s.at[0], wo_r.at[4], L.yn)
 
     wo_b.start()
     wo_a.start()
@@ -413,6 +421,7 @@
         keep[k].start()
         share_own(k, 0)
     late = [pltpu.make_async_copy(gate, gv, ld_s.at[5]), pltpu.make_async_copy(stream, mid, ld_s.at[8])]
+    late += [pltpu.make_async_copy(head_gain, gain_h, ld_s.at[9]), pltpu.make_async_copy(mix_gain, gain_m, ld_s.at[10])]
     for cp in late:
         cp.start()
 
@@ -492,7 +501,7 @@
     before[y] = jnp.where(is0, whole, onto).astype(bf16)
     back = remote(bsend, before.at[y], s_s.at[1], s_r.at[1], L.yn)
     back.start()
-    wo_from_b = remote(out_w.at[wo_rows(y), :], wo.at[L.xn[1], wo_rows(y), :], wo_s.at[3], wo_r.at[3], L.xn)
+    wo_from_b = remote(out_w.at[wo_rows(y), :], wo.at[L.xn[1], wo_rows(y), :], wo_s.at[0], wo_r.at[3], L.xn)
     wo_from_b.wait_recv()
     wo_pass(y).start()
     cross[1].start()
@@ -503,7 +512,8 @@
     forward_inner(0, 2, y)
     remote(bsend, before.at[1 - y], s_s.at[1], s_r.at[1], L.yn).wait_recv()
     late[0].wait()
-    gain = head_gain[...]
+    late[2].wait()
+    gain = gain_h[...]
 
     def finish(t):
         for r in range(0, rows, 128):
@@ -515,13 +525,11 @@
                 g = gv[at, vs].astype(f32)
                 heads[t, pl.ds(r, 128), vs] = (scaled * gain * (g / (1.0 + jnp.exp(-g)))).astype(bf16)
 
-    head_sends = []
-    for i, dev in enumerate((L.xn, L.xo, L.core)):
+    for dev in (L.xn, L.xo, L.core):
         t = dev[1]
         finish(t)
-        cp = remote(heads.at[t], hrecv.at[L.tp], h_s.at[i], h_r.at[i], dev)
+        cp = remote(heads.at[t], hrecv.at[L.tp], h_s.at[0], h_r.at[0], dev)
         cp.start()
-        head_sends.append(cp)
     finish(L.tp)
     hrecv[L.tp] = heads[L.tp]
     forward_inner(0, 1, 1 - y)
@@ -529,17 +537,19 @@
 
     remote(out_w.at[wo_rows(None), :], wo.at[L.xn[1], wo_rows(None), :], wo_s.at[0], wo_r.at[0], L.xn).wait_recv()
     wo_pass(1 - y).wait_recv()
-    relay = remote(wo.at[L.xn[1]], wo.at[L.xn[1]], wo_s.at[2], wo_r.at[2], L.core)
+    relay = remote(wo.at[L.xn[1]], wo.at[L.xn[1]], wo_s.at[0], wo_r.at[2], L.core)
     relay.start()
-    remote(out_w, wo.at[L.core[1]], wo_s.at[1], wo_r.at[1], L.core).wait_recv()
-    remote(wo.at[L.xo[1]], wo.at[L.xo[1]], wo_s.at[2], wo_r.at[2], L.core).wait_recv()
+    remote(out_w, wo.at[L.core[1]], wo_s.at[0], wo_r.at[1], L.core).wait_recv()
+    remote(wo.at[L.xo[1]], wo.at[L.xo[1]], wo_s.at[0], wo_r.at[2], L.core).wait_recv()
     wo_own.wait()
     late[1].wait()
+    late[3].wait()
     forward_inner(0, 3, y)
     arrive_edge(0, 1, y)
     arrive_edge(0, 1, 1 - y)
-    for i, dev in enumerate((L.xn, L.xo, L.core)):
-        remote(heads.at[dev[1]], hrecv.at[dev[1]], h_s.at[i], h_r.at[i], dev).wait_recv()
+    others = pl.ds(0, n_tp - 1)
+    all_heads = remote(heads.at[others], hrecv.at[others], h_s.at[0], h_r.at[0], L.xn)
+    all_heads.wait_recv()
 
     square = jnp.zeros((rows, 1), f32)
     wide = min(512, width)
@@ -555,14 +565,14 @@
     norm = lax.rsqrt(square * (1.0 / width) + EPS)
     for n in range(0, width, wide):
         cols = pl.ds(n, wide)
-        acts[:rows, cols] = (mid[:, cols].astype(f32) * norm * mix_gain[:, cols]).astype(bf16)
+        acts[:rows, cols] = (mid[:, cols].astype(f32) * norm * gain_m[:, cols]).astype(bf16)
 
     a, b = pl.ds(0, half_rows), pl.ds(half_rows, half_rows)
 
     def act_copy(i):
         slot, part, dst, dev = [(0, 0, 1, L.xn), (0, 1, 1, L.xn), (0, 0, 2, L.yn), (0, 1, 2, L.yn), (1, 0, 3, L.yn), (2, 1, 3, L.xn)][i]
         src = acts.at[pl.ds(slot * rows + part * half_rows, half_rows), :]
-        return remote(src, acts.at[pl.ds(dst * rows + part * half_rows, half_rows), :], a_s.at[i], a_r.at[i], dev)
+        return remote(src, acts.at[pl.ds(dst * rows + part * half_rows, half_rows), :], a_s.at[0], a_r.at[i], dev)
 
     for i in (0, 3, 1, 2):
         act_copy(i).start()
@@ -587,9 +597,8 @@
     arrive_edge(0, 3, y)
     arrive_edge(0, 3, 1 - y)
     keep[0].wait()
-    for j in range(nz):
-        for part in range(2):
-            from_core(0, j, part).wait_recv()
+    theirs = up.at[:, pl.ds(pl.multiple_of((1 - c) * half, half), half)]
+    remote(theirs, theirs, d_s.at[0], du_r.at[0], L.core).wait_recv()
 
     def up_step(n, carry):
         at = pl.ds(pl.multiple_of(n * UP_TILE, UP_TILE), UP_TILE)
@@ -603,7 +612,6 @@
     keep[1].wait()
 
     steps = 2 * nz * CUT
-    final = steps - CUT
 
     def columns(u, n=1):
         d = (L.piece(u // (2 * CUT)) * 2 * CUT + u % (2 * CUT)) * fine
@@ -619,7 +627,7 @@
             (psend.at[0, a, cols], sum_x.at[a, cols], L.xn),
             (psend.at[1, b, cols], sum_y.at[b, cols], L.yn),
         ][i]
-        return remote(src, dst, p_s.at[i, u], p_r.at[i, u], dev)
+        return remote(src, dst, p_s.at[0], p_r.at[0 if i < 2 else 1, u], dev)
 
     def terms_of(u, n):
         s = u // (2 * CUT)
@@ -629,8 +637,8 @@
             for k in range(n):
                 arrive(1, s, u % (2 * CUT) + k, False)
 
-        for k in range(n):
-            from_core(1, L.piece(s), u % (2 * CUT) + k).wait_recv()
+        theirs = down.at[columns(u, n), pl.ds(pl.multiple_of((1 - c) * half, half), half)]
+        remote(theirs, theirs, d_s.at[1], core_r(1, s, u % (2 * CUT)), L.core).wait_recv()
         cols = columns(u, n)
         terms = lax.dot_general(hidden[...], down[cols, :], NT, preferred_element_type=f32)
         pown[:, cols] = terms[:rows]
@@ -642,17 +650,17 @@
 
     def pass_on(u):
         cols = columns(u)
-        part_copy(0, u).wait_recv()
+        passed = psend.at[0, :, cols]
+        remote(passed, passed, p_s.at[0], p_r.at[0, u], L.xn).wait_recv()
         psend[0, a, cols] = (psend[0, a, cols].astype(f32) + pass_y[:, cols].astype(f32)).astype(bf16)
         part_copy(4, u).start()
-        part_copy(1, u).wait_recv()
         psend[1, b, cols] = (psend[1, b, cols].astype(f32) + pass_x[:, cols].astype(f32)).astype(bf16)
         part_copy(5, u).start()
 
     def close(u):
         cols = columns(u)
-        for i in (2, 3, 4, 5):
-            part_copy(i, u).wait_recv()
+        sums = psend.at[pl.ds(0, 2), :, cols]
+        remote(sums, sums, p_s.at[0], p_r.at[1, u], L.xn).wait_recv()
         feed = pown[:, cols] + sum_x[:, cols].astype(f32) + sum_y[:, cols].astype(f32)
         out[:, cols] = (mid[:, cols].astype(f32) + feed).astype(bf16)
 
@@ -677,32 +685,32 @@
 
     lax.fori_loop(0, steps + 2 * CUT, down_step, 0)
 
+    def sent(ref, sem):
+        remote(ref, ref, sem, sem, L.core).wait_send()
+
+    mine_cols = pl.ds(0, half)
+    sent(up.at[pl.ds(0, 2 * slab), mine_cols], y_s.at[0])
+    for side in range(2):
+        @pl.when((z < nz - 1) if side else (z > 0))
+        def _():
+            sent(up.at[pl.ds(0, 4 * slab), mine_cols], zown_s.at[side])
     for k in range(2):
-        cross[k].wait_send()
-        for far in range(2):
-            for side in range(2):
-                @pl.when((z < nz - 1) if side else (z > 0))
-                def _():
-                    for cut in range(cuts[k]):
-                        to_side(k, far, cut, side).wait_send()
-        for part in range(2 * cuts[k]):
-            for s in range(nz):
-                j = L.piece(s)
-                to_core(k, j, part).wait_send()
-                if s:
-                    @pl.when(inner)
-                    def _():
-                        onward(k, j, part).wait_send()
-    for cp in [wo_a, wo_b, wo_c, wo_pass(y), relay, swap, back] + head_sends + [act_copy(i) for i in range(6)]:
-        cp.wait_send()
+        sent(up.at[:, mine_cols], d_s.at[k])
+
+        @pl.when(inner)
+        def _():
+            sent(up.at[pl.ds(0, 2 * slab * (nz - 1)), mine_cols], zfwd_s.at[k])
+    sent(wo.at[pl.ds(0, 3)], wo_s.at[0])
+    swap.wait_send()
+    back.wait_send()
 
     @pl.when(z < nz - 1)
     def _():
         hand_on(z + 1).wait_send()
 
-    for u in range(steps):
-        for i in range(6):
-            part_copy(i, u).wait_send()
+    all_heads.wait_send()
+    sent(acts.at[pl.ds(0, 3 * rows), :], a_s.at[0])
+    sent(psend, p_s.at[0])
 
 
 def fused(
@@ -720,7 +728,7 @@
     return pl.pallas_call(
         functools.partial(layer_kernel, n_sp, n_tp),
         out_shape=pltpu.VMEM((rows, width), bf16),
-        in_specs=[hbm] * 6 + [vmem] * 2 + [hbm] * 3,
+        in_specs=[hbm] * 11,
         out_specs=vmem,
         scratch_shapes=[
             V((width, 2 * half), bf16), V((width, 2 * half), bf16), V((n_tp, out_w.shape[0], width), bf16),
@@ -732,10 +740,9 @@
             V((4 * rows, width), bf16), V((4 * rows, 2 * half), bf16), V((rows, width), bf16),
             V((3, rows, width), bf16), V((rows, width), f32), V((rows, width), bf16), V((rows, width), bf16),
             V((rows // 2, width), bf16), V((rows // 2, width), bf16),
-            D((9,)), D((2, 2, CUT, 2)), D((2, nz, 2 * CUT)), D((2, nz, 2 * CUT)), D((2,)), D((2,)), D((2, nz, 2 * CUT)),
-            D((2, nz, 2 * CUT)),
-            D((5,)), D((5,)), D((2,)), D((2,)), D((1,)), D((1,)), D((3,)), D((3,)), D((6,)), D((6,)),
-            D((6, np_)), D((6, np_)),
+            V((1, head_gain.shape[0]), f32), V((1, width), f32),
+            D((11,)), D((2,)), D((2,)), D((nz, 2 + 2 * CUT)), D((1,)), D((2,)), D((2,)), D((1,)), D((2 * nz - 1 + CUT,)),
+            D((1,)), D((5,)), D((2,)), D((2,)), D((1,)), D((1,)), D((1,)), D((1,)), D((1,)), D((6,)), D((1,)), D((2, np_)),
         ],
         compiler_params=pltpu.CompilerParams(
             collective_id=0, has_side_effects=True, vmem_limit_bytes=58_000_000

time: 154 us -> 151 us (0.981)
  Pallas kernels: 153 us -> 150 us
    pallas_call x1, Pallas kernels: 153 us -> 150 us  [fused(): pl.pallas_call(functools.partial(layer_kernel, n_sp, n_tp), out_shape=plt...]
where the time goes in v2:
time: 151 us
  Pallas kernels  150 us (99%)
    pallas_call x1, Pallas kernels, fused(): pl.pallas_call(functools.partial(layer_kernel, n_sp, n_tp), out_shape=plt...  150 us

profile of v2, /device:TPU:0, one launch (start us, length us, event | category | flops | bytes accessed | tf_op | source)
XLA Modules:
  0.0 150.5 jit_solution(6516296853150533647)
XLA Ops:
  0.0 149.6 %layer.1 = bf16[256,2048]{1,0:T(8,128)(2,1)S(1)} custom-call(bf16[256,2048]{1,0:T(8,128)(2,1)} %stream.1, bf16[1024,256]{1,0:T(8,128)(2,1)} %query.1, bf16[1024,256]{1,0:T(8,128)(2,1)} %key.1, bf16[1024,512]{1,0:T(8,128)(2,1)} %value.1, bf16[1024,512]{1,0:T(8,128)(2,1)} %gate.1, f32[1024,256]{1,0:T(8,128)} %rates_in.1, f32[1,256]{1,0:T(1,128)} %bitcast.3, ...), custom_call_target="tpu_custom_call" | custom-call | tf_op jit(solution)/shard_map/layer/pallas_call | solution.py:728
  149.6 1.0 copy.13

commit v3 on v2

--- a/solution.py
+++ b/solution.py
@@ -572,7 +572,7 @@
     def act_copy(i):
         slot, part, dst, dev = [(0, 0, 1, L.xn), (0, 1, 1, L.xn), (0, 0, 2, L.yn), (0, 1, 2, L.yn), (1, 0, 3, L.yn), (2, 1, 3, L.xn)][i]
         src = acts.at[pl.ds(slot * rows + part * half_rows, half_rows), :]
-        return remote(src, acts.at[pl.ds(dst * rows + part * half_rows, half_rows), :], a_s.at[0], a_r.at[i], dev)
+        return remote(src, acts.at[pl.ds(dst * rows + part * half_rows, half_rows), :], a_s.at[0], a_r.at[(0, 2, 2, 1, 2, 2)[i]], dev)
 
     for i in (0, 3, 1, 2):
         act_copy(i).start()
@@ -589,8 +589,8 @@
             forward_inner(1, s, part)
     arrive_edge(0, 2, y)
     arrive_edge(0, 2, 1 - y)
-    for i in (1, 2, 4, 5):
-        act_copy(i).wait_recv()
+    rest = acts.at[pl.ds(0, 2 * rows), :]
+    remote(rest, rest, a_s.at[0], a_r.at[2], L.xn).wait_recv()
     for part in range(CUT):
         forward_inner(1, 3, part)
 
@@ -637,10 +637,16 @@
             for k in range(n):
                 arrive(1, s, u % (2 * CUT) + k, False)
 
-        theirs = down.at[columns(u, n), pl.ds(pl.multiple_of((1 - c) * half, half), half)]
+        cols = columns(u, n)
+        got_here, got_there = (pl.ds(pl.multiple_of(k * half, half), half) for k in (c, 1 - c))
+
+        def product(units):
+            return lax.dot_general(hidden[:, units], down[cols, units], NT, preferred_element_type=f32)
+
+        terms = product(got_here) if n == 1 else None
+        theirs = down.at[cols, got_there]
         remote(theirs, theirs, d_s.at[1], core_r(1, s, u % (2 * CUT)), L.core).wait_recv()
-        cols = columns(u, n)
-        terms = lax.dot_general(hidden[...], down[cols, :], NT, preferred_element_type=f32)
+        terms = product(pl.ds(0, 2 * half)) if terms is None else terms + product(got_there)
         pown[:, cols] = terms[:rows]
         for i in range(3):
             psend[i, :, cols] = terms[(i + 1) * rows : (i + 2) * rows].astype(bf16)
@@ -664,26 +670,26 @@
         feed = pown[:, cols] + sum_x[:, cols].astype(f32) + sum_y[:, cols].astype(f32)
         out[:, cols] = (mid[:, cols].astype(f32) + feed).astype(bf16)
 
+    def passed_after(u):
+        return jnp.where(u < final - 1, jnp.maximum(u - CUT + 1, 0), jnp.where(u < steps - 1, final, steps))
+
+    def closed_after(u):
+        return jnp.where(u < final, jnp.maximum(u - 2 * CUT + 1, 0), jnp.where(u < steps - 1, final, steps))
+
     def down_step(u, carry):
         @pl.when(jnp.logical_and(u < final, u % CUT == 0))
         def _():
             terms_of(u, CUT)
 
-        @pl.when(jnp.logical_and(u >= final, u < steps))
+        @pl.when(u >= final)
         def _():
             terms_of(u, 1)
 
-        @pl.when(jnp.logical_and(u >= CUT, u < steps + CUT))
-        def _():
-            pass_on(u - CUT)
-
-        @pl.when(u >= 2 * CUT)
-        def _():
-            close(u - 2 * CUT)
-
+        lax.fori_loop(passed_after(u - 1), passed_after(u), lambda v, _: pass_on(v), None)
+        lax.fori_loop(closed_after(u - 1), closed_after(u), lambda v, _: close(v), None)
         return carry
 
-    lax.fori_loop(0, steps + 2 * CUT, down_step, 0)
+    lax.fori_loop(0, steps, down_step, 0)
 
     def sent(ref, sem):
         remote(ref, ref, sem, sem, L.core).wait_send()
@@ -742,7 +748,7 @@
             V((rows // 2, width), bf16), V((rows // 2, width), bf16),
             V((1, head_gain.shape[0]), f32), V((1, width), f32),
             D((11,)), D((2,)), D((2,)), D((nz, 2 + 2 * CUT)), D((1,)), D((2,)), D((2,)), D((1,)), D((2 * nz - 1 + CUT,)),
-            D((1,)), D((5,)), D((2,)), D((2,)), D((1,)), D((1,)), D((1,)), D((1,)), D((1,)), D((6,)), D((1,)), D((2, np_)),
+            D((1,)), D((5,)), D((2,)), D((2,)), D((1,)), D((1,)), D((1,)), D((1,)), D((1,)), D((3,)), D((1,)), D((2, np_)),
         ],
         compiler_params=pltpu.CompilerParams(
             collective_id=0, has_side_effects=True, vmem_limit_bytes=58_000_000

time: 151 us -> 151 us (level)
  no operation moved by 1% of the time
where the time goes in v3:
time: 151 us
  Pallas kernels  150 us (99%)
    pallas_call x1, Pallas kernels, fused(): pl.pallas_call(functools.partial(layer_kernel, n_sp, n_tp), out_shape=plt...  150 us

profile of v3, /device:TPU:0, one launch (start us, length us, event | category | flops | bytes accessed | tf_op | source)
XLA Modules:
  0.0 151.1 jit_solution(13860428323743466158)
XLA Ops:
  0.0 150.2 %layer.1 = bf16[256,2048]{1,0:T(8,128)(2,1)S(1)} custom-call(bf16[256,2048]{1,0:T(8,128)(2,1)} %stream.1, bf16[1024,256]{1,0:T(8,128)(2,1)} %query.1, bf16[1024,256]{1,0:T(8,128)(2,1)} %key.1, bf16[1024,512]{1,0:T(8,128)(2,1)} %value.1, bf16[1024,512]{1,0:T(8,128)(2,1)} %gate.1, f32[1024,256]{1,0:T(8,128)} %rates_in.1, f32[1,256]{1,0:T(1,128)} %bitcast.3, ...), custom_call_target="tpu_custom_call" | custom-call | tf_op jit(solution)/shard_map/layer/pallas_call | solution.py:734
  150.2 1.0 copy.13
